TPU v7x, 32 devices: a whole 2x2x4 slice. The times are simulated.
32 devices in a mesh: ep: 8 (over z, y), tp: 4 (over x, core).
Axes of the slice: x: 2, y: 2, z: 4, core: 2. Of those that a mesh axis runs over, the one named last changes fastest.
Arguments:
- q_heads: bfloat16 [8192, 1024], P('ep', 'tp'), may hold values from -200 to 200
- k_heads: bfloat16 [8192, 256], P('ep', 'tp'), may hold values from -6 to 6
- v_heads: bfloat16 [8192, 256], P('ep', 'tp'), may hold values from -6 to 6
- sink_logits: float32 [16], P('tp'), may hold values from 1 to 5
- out_weight: bfloat16 [1024, 2048], P(None, 'tp'), may hold values from -1.5 to 1.5
- tokens_b: bfloat16 [4096, 2048], P('ep'), may hold values from -6 to 6
- moe_gain: float32 [2048], replicated, may hold values from 0.1 to 1.9
- router_group: bfloat16 [2048, 4], replicated, may hold values from -0.125 to 0.125
- router_expert: bfloat16 [2048, 16], replicated, may hold values from -0.125 to 0.125
- route_expert: int32 [4096, 2], P('ep'), may hold values from 0 to 15, as said below
- expert_gate: bfloat16 [16, 2048, 1024], P('ep', None, 'tp'), may hold values from -0.125 to 0.125
- expert_up: bfloat16 [16, 2048, 1024], P('ep', None, 'tp'), may hold values from -0.125 to 0.125
- expert_down: bfloat16 [16, 1024, 2048], P('ep', 'tp'), may hold values from -0.75 to 0.75
Outputs:
- mixer_out: bfloat16 [8192, 2048], P('ep', 'tp')
- moe_out: bfloat16 [4096, 2048], P(('ep', 'tp'))
Inputs may be any that keep to these rules, and one draw needn't show every extreme that they name: `route_expert`: each token names two different experts, in rising order, of one group of 4 consecutive experts. In each aligned block of 128 rows (the rows of one device) no expert is named by more than 32 tokens, in each group one expert is named by exactly 32 tokens of every block, and each group is named by a quarter of every block's tokens.
All inputs are finite; a program needn't handle non-finite values.
Results may differ from a plain program's by a relative error of at most 0.011.
Values may be sent and summed in bfloat16 or wider, within the bound.
No kernel may reach another device: no remote copies, remote signals or barrier semaphores. Data moves between devices by JAX's collectives and lax.ppermute only.
A program may use at most 128 MiB of HBM per device.

v0:
```python
import jax
import jax.numpy as jnp
from jax import lax
from jax.sharding import PartitionSpec as P

HEADS = 16
KV = 4
HD = 64
WINDOW = 128


def shifted(value, axis, steps):
    count = lax.axis_size(axis)
    leading, last = (max(0, -steps), min(count, count - steps))
    return lax.ppermute(value, axis, [(source, source + steps) for source in range(leading, last)])


def normalize(rows_in, gain):
    values = rows_in.astype(jnp.float32)
    scaled = values * lax.rsqrt(jnp.mean(values * values, axis=-1, keepdims=True) + 1e-06) * gain
    return scaled.astype(jnp.bfloat16)


def gate_weights(normed, routes, router_group, router_expert):
    group_logits = jnp.dot(normed, router_group, preferred_element_type=jnp.float32)
    expert_logits = jnp.dot(normed, router_expert, preferred_element_type=jnp.float32)
    group_count = router_group.shape[1]
    expert_count = router_expert.shape[1]
    chosen_group = routes[:, 0] // (expert_count // group_count)
    group_match = chosen_group[:, None] == jnp.arange(group_count, dtype=jnp.int32)[None, :]
    group_share = jnp.sum(
        jnp.where(group_match, jax.nn.softmax(group_logits, axis=-1), 0.0), axis=-1
    )
    expert_match = routes[:, :, None] == jnp.arange(expert_count, dtype=jnp.int32)[None, None, :]
    picked = jnp.sum(jnp.where(expert_match, expert_logits[:, None, :], 0.0), axis=-1)
    return group_share[:, None] * jax.nn.softmax(picked, axis=-1)


def slot_positions(routes, sub_count, expert_count):
    flat_routes = routes.reshape(sub_count, -1)
    onehot = (
        flat_routes[:, :, None] == jnp.arange(expert_count, dtype=jnp.int32)[None, None, :]
    ).astype(jnp.int32)
    places = jnp.sum(onehot * jnp.cumsum(onehot, axis=1), axis=2) - 1
    return (flat_routes, places)


def fill_slots(normed, flat_routes, places, sub_count, expert_count, capacity, exp_local):
    sub_index = jnp.arange(sub_count, dtype=jnp.int32)[:, None]
    target = ((flat_routes * sub_count + sub_index) * capacity + places).reshape(-1)
    source = jnp.repeat(normed, 2, axis=0)
    buffer = jnp.zeros((expert_count * sub_count * capacity, normed.shape[1]), jnp.bfloat16)
    buffer = buffer.at[target].set(source)
    return buffer.reshape(
        expert_count // exp_local, exp_local, sub_count, capacity, normed.shape[1]
    )


def per_device(
    q_heads,
    k_heads,
    v_heads,
    sink_logits,
    out_weight,
    tokens_b,
    moe_gain,
    router_group,
    router_expert,
    route_expert,
    expert_gate,
    expert_up,
    expert_down,
):
    span_len = WINDOW
    row_count = q_heads.shape[0]
    kv_local = k_heads.shape[1] // HD
    group_size = HEADS // KV
    blocks = row_count // span_len
    stacked = jnp.stack([k_heads[row_count - span_len :], v_heads[row_count - span_len :]])
    earlier = shifted(stacked, "ep", 1)

    def make_band(own_rows, prev_rows):
        extended = jnp.concatenate([prev_rows, own_rows], axis=0).reshape(
            blocks + 1, span_len, kv_local, HD
        )
        return jnp.concatenate([extended[:-1], extended[1:]], axis=1)

    key_band = make_band(k_heads, earlier[0])
    value_band = make_band(v_heads, earlier[1])
    query_blocks = q_heads.reshape(blocks, span_len, kv_local, group_size, HD)
    scores = jnp.einsum(
        "nqhgd,nkhd->nhgqk", query_blocks, key_band, preferred_element_type=jnp.float32
    ) * HD ** (-0.5)
    first_row = lax.axis_index("ep") * row_count
    query_index = jnp.arange(span_len, dtype=jnp.int32)[:, None]
    key_index = jnp.arange(2 * span_len, dtype=jnp.int32)[None, :]
    distance = query_index + span_len - key_index
    key_place = (
        first_row
        + jnp.arange(blocks, dtype=jnp.int32)[:, None, None] * span_len
        + key_index[None]
        - span_len
    )
    allowed = (distance >= 0)[None] & (distance < span_len)[None] & (key_place >= 0)
    masked = jnp.where(allowed[:, None, None], scores, -1e30)
    sink_full = sink_logits.reshape(kv_local, group_size)[None, :, :, None]
    row_max = jnp.maximum(jnp.max(masked, axis=-1), sink_full)
    weights_exp = jnp.exp(masked - row_max[..., None])
    denominator = jnp.sum(weights_exp, axis=-1) + jnp.exp(sink_full - row_max)
    probs = (weights_exp / denominator[..., None]).astype(jnp.bfloat16)
    attended = jnp.einsum(
        "nhgqk,nkhd->nqhgd", probs, value_band, preferred_element_type=jnp.float32
    )
    attended = attended.astype(jnp.bfloat16).reshape(row_count, kv_local * group_size * HD)
    mixed = jnp.dot(
        lax.all_gather(attended, "tp", axis=1, tiled=True),
        out_weight,
        preferred_element_type=jnp.float32,
    )
    mixer_out = mixed.astype(jnp.bfloat16)
    tp_count = lax.axis_size("tp")
    tp_index = lax.axis_index("tp")
    exp_local = expert_gate.shape[0]
    expert_count = exp_local * lax.axis_size("ep")
    rows_dev = tokens_b.shape[0] // tp_count
    capacity = min(4 * rows_dev // expert_count, rows_dev // 4)
    own_routes = lax.dynamic_slice_in_dim(route_expert, tp_index * rows_dev, rows_dev, 0)
    own_normed = normalize(
        lax.dynamic_slice_in_dim(tokens_b, tp_index * rows_dev, rows_dev, 0), moe_gain
    )
    flat_routes, places = slot_positions(own_routes, 1, expert_count)
    buffer = fill_slots(own_normed, flat_routes, places, 1, expert_count, capacity, exp_local)
    delivered = lax.all_to_all(buffer, "ep", split_axis=0, concat_axis=0, tiled=True)
    arrived = lax.all_gather(delivered, "tp", axis=2, tiled=True)
    own_flat = flat_routes[0]
    own_places = places[0]
    gates = gate_weights(own_normed, own_routes, router_group, router_expert)
    gate_pre = jnp.einsum(
        "setcd,edf->setcf", arrived, expert_gate, preferred_element_type=jnp.float32
    )
    up_pre = jnp.einsum("setcd,edf->setcf", arrived, expert_up, preferred_element_type=jnp.float32)
    activated = (jax.nn.silu(gate_pre) * up_pre).astype(jnp.bfloat16)
    partial_value = jnp.einsum(
        "setcf,efd->setcd", activated, expert_down, preferred_element_type=jnp.float32
    )
    summed = lax.psum_scatter(
        partial_value.astype(jnp.bfloat16), "tp", scatter_dimension=2, tiled=True
    )
    returned = lax.all_to_all(summed, "ep", split_axis=0, concat_axis=0, tiled=True)
    returned = returned.reshape(expert_count * capacity, returned.shape[-1])
    picked_rows = returned[own_flat * capacity + own_places].reshape(
        rows_dev, 2, returned.shape[-1]
    )
    moe_out = jnp.sum(gates[:, :, None] * picked_rows.astype(jnp.float32), axis=1).astype(
        jnp.bfloat16
    )
    return (mixer_out, moe_out)


def solution(mesh):
    in_specs = (
        P("ep", "tp"),
        P("ep", "tp"),
        P("ep", "tp"),
        P("tp"),
        P(None, "tp"),
        P("ep", None),
        P(),
        P(),
        P(),
        P("ep", None),
        P("ep", None, "tp"),
        P("ep", None, "tp"),
        P("ep", "tp", None),
    )
    out_specs = (P("ep", "tp"), P(("ep", "tp"), None))
    return jax.shard_map(
        per_device, mesh=mesh, in_specs=in_specs, out_specs=out_specs, check_vma=False
    )
```

profile of v0, /device:TPU:0, one launch (start us, length us, event | category | flops | bytes accessed | tf_op | source)
XLA Modules:
  0.0 384.7 jit_solution(17518008943013169215)
XLA Ops:
  9.7 1.2 fusion.24
  10.9 1.3 fusion.26
  12.2 1.6 broadcast_in_dim.34
  13.8 2.3 reshape.383
  16.0 4.4 %scatter_custom_fusion = bf16[512,2048]{1,0:T(8,128)(2,1)} fusion(s32[256]{0:T(256)S(1)} %bitcast.171, bf16[256,2048]{1,0:T(8,128)(2,1)} %reshape.383, bf16[]{:T(256)} %constant.67.clone.1), kind=kCustom, calls=%fused_computation.35 | custom fusion | bytes 2097664 | tf_op jit(solution)/shard_map/scatter | solution.py:53
  20.5 55.5 %all_to_all.10 = bf16[8,2,1,32,2048]{4,3,2,1,0:T(8,128)(2,1)S(1)} all-to-all(bf16[8,2,1,32,2048]{4,3,2,1,0:T(8,128)(2,1)} %bitcast.159), channel_id=1, replica_groups=mesh['ep'=8,'tp'=4] {'ep'}, dimensions={0} | all-to-all | bytes 4194304 | tf_op jit(solution)/shard_map/all_to_all | solution.py:133
  76.0 1.5 copy.69
  77.6 57.4 %all-gather.5.cloned.1.call-done = bf16[8,2,4,32,2048]{4,3,2,0,1:T(8,128)(2,1)} async-done(((bf16[8,2,1,32,2048]{4,3,2,0,1:T(8,128)(2,1)}), bf16[8,2,4,32,2048]{4,3,2,0,1:T(8,128)(2,1)}) %all-gather.5.cloned.1.call-update) | async-done | bytes 8388624 | tf_op jit(solution)/shard_map/all_gather | solution.py:134
  134.9 7.7 %fusion.3 = f32[2,8,4,32,256]{4,3,2,1,0:T(8,128)} fusion(bf16[8,2,4,32,2048]{4,3,2,0,1:T(8,128)(2,1)} %all-gather.5.cloned.1.call-done, bf16[2,2048,256]{2,1,0:T(8,128)(2,1)} %param.24), kind=kOutput, calls=%fused_computation.9 | convolution fusion | flops 2147483648 | bytes 12582912 | tf_op jit(solution)/shard_map/setcd,edf->setcf/dot_general | solution.py:141
  142.6 13.5 %convert_bitcast_fusion = bf16[8,2,4,32,2048]{4,3,2,0,1:T(8,128)(2,1)} fusion(bf16[2,256,2048]{2,1,0:T(8,128)(2,1)S(1)} %copy-done, f32[2,8,4,32,256]{4,3,2,1,0:T(8,128)} %fusion.3, bf16[8,2,4,32,2048]{4,3,2,0,1:T(8,128)(2,1)} %all-gather.5.cloned.1.call-done, bf16[2,2048,256]{2,1,0:T(8,128)(2,1)} %param.23), kind=kOutput, calls=%fused_computation.2 | convolution fusion | flops 4302307328 | bytes 23068672 | tf_op jit(solution)/shard_map/setcf,efd->setcd/dot_general | solution.py:143
  157.1 3.6 collective-permute-start
  162.5 0.9 fusion.1
  163.5 1.1 fusion
  165.4 143.8 %all-reduce.3.cloned.1.call-done = bf16[8,2,4,32,2048]{4,3,2,0,1:T(8,128)(2,1)} async-done(((bf16[8,2,4,32,2048]{4,3,2,0,1:T(8,128)(2,1)}), bf16[8,2,4,32,2048]{4,3,2,0,1:T(8,128)(2,1)}) %all-reduce.3.cloned.1.call-update) | async-done | bytes 8388624
  309.2 2.5 constant_dynamic-slice_fusion
  311.6 1.6 copy.70
  313.2 5.5 %all-to-all-start.1 = ((bf16[8,2,1,32,2048]{4,3,2,1,0:T(8,128)(2,1)}), bf16[8,2,1,32,2048]{4,3,2,1,0:T(8,128)(2,1)S(1)}, u32[]{:S(2)}, u32[]{:S(2)}) async-start(bf16[8,2,1,32,2048]{4,3,2,1,0:T(8,128)(2,1)} %copy.70), calls=%async_computation.1 | async-start | bytes 4194304 | tf_op jit(solution)/shard_map/all_to_all | solution.py:149
  318.8 3.4 fusion.21
  324.3 22.5 %all-gather.3.cloned.1.call-done = bf16[1024,1024]{0,1:T(8,128)(2,1)} async-done(((bf16[1024,256]{0,1:T(8,128)(2,1)}), bf16[1024,1024]{0,1:T(8,128)(2,1)}) %all-gather.3.cloned.1.call-update) | async-done | bytes 2097168 | tf_op jit(solution)/shard_map/all_gather | solution.py:116
  346.8 4.1 %convolution_convert_fusion = bf16[1024,512]{1,0:T(8,128)(2,1)} fusion(bf16[1024,1024]{0,1:T(8,128)(2,1)} %all-gather.3.cloned.1.call-done, bf16[1024,512]{1,0:T(8,128)(2,1)} %param.17), kind=kOutput, calls=%fused_computation.24 | convolution fusion | flops 1074266112 | bytes 4194304 | tf_op jit(solution)/shard_map/dot_general | solution.py:115
  350.9 15.8 %all-to-all-done.1 = bf16[8,2,1,32,2048]{4,3,2,1,0:T(8,128)(2,1)S(1)} async-done(((bf16[8,2,1,32,2048]{4,3,2,1,0:T(8,128)(2,1)}), bf16[8,2,1,32,2048]{4,3,2,1,0:T(8,128)(2,1)S(1)}, u32[]{:S(2)}, u32[]{:S(2)}) %all-to-all-start.1) | async-done | bytes 2097184 | tf_op jit(solution)/shard_map/all_to_all | solution.py:149
  366.7 2.3 gather_fusion
  369.0 3.5 reshape.370
  372.6 5.6 %multiply_reduce_fusion = bf16[128,2048]{1,0:T(8,128)(2,1)} fusion(f32[128,2,2048]{2,1,0:T(2,128)} %reshape.370, f32[128,2]{1,0:T(8,128)S(1)} %copy.62), kind=kLoop, calls=%fused_computation.22 | loop fusion | flops 786432 | bytes 2622464 | tf_op jit(solution)/shard_map/reduce_sum | solution.py:154
  (80 shorter events, 8.1 us)
Async XLA Ops:
  7.2 135.4 %copy-start = (bf16[2,256,2048]{2,1,0:T(8,128)(2,1)S(1)}, bf16[2,256,2048]{2,1,0:T(8,128)(2,1)}, u32[]{:S(2)}) copy-start(bf16[2,256,2048]{2,1,0:T(8,128)(2,1)} %param.25) | copy-start | bytes 6291460
  7.2 127.8 %all-gather.5.cloned.1.call-start = ((), (), s32[]{:S(2)}) async-start(), calls=%async_computation.3 | async-start | bytes 10485760 | tf_op jit(solution)/shard_map/all_gather | solution.py:134
  77.5 231.6 %all-reduce.3.cloned.1.call-start = ((), (), s32[]{:S(2)}) async-start(), calls=%async_computation.4 | async-start | bytes 16777216
  156.1 0.9 copy-start.3
  156.1 1.0 copy-start.4
  156.1 5.1 %copy-start.5 = (bf16[1024,256]{1,0:T(8,128)(2,1)S(1)}, bf16[1024,256]{1,0:T(8,128)(2,1)}, u32[]{:S(2)}) copy-start(bf16[1024,256]{1,0:T(8,128)(2,1)} %param.13) | copy-start | bytes 1572868
  157.1 4.6 %copy-start.9 = (u32[32]{0:T(128)S(1)}, u32[32]{0:T(128)}, u32[]{:S(2)}) copy-start(u32[32]{0:T(128)} %constant.75) | copy-start | bytes 388
  157.1 5.2 %collective-permute-start = (bf16[2,128,64]{1,2,0:T(8,128)(2,1)S(1)}, bf16[2,128,64]{1,2,0:T(8,128)(2,1)S(1)}, u32[]{:S(2)}, u32[]{:S(2)}) collective-permute-start(bf16[2,128,64]{1,2,0:T(8,128)(2,1)S(1)} %pad_maximum_fusion.2), channel_id=1, source_target_pairs={{0,4},{4,8},{8,12},{12,16},{16,20},{20,24},{24,28},{1,5},{5,9},{9,... | collective-permute-start | bytes 98312 | tf_op jit(solution)/shard_map/ppermute | solution.py:15
  162.5 0.9 copy-start.8
  163.4 1.9 copy-start.2
  313.2 53.4 %all-to-all-start.1 = ((bf16[8,2,1,32,2048]{4,3,2,1,0:T(8,128)(2,1)}), bf16[8,2,1,32,2048]{4,3,2,1,0:T(8,128)(2,1)S(1)}, u32[]{:S(2)}, u32[]{:S(2)}) async-start(bf16[8,2,1,32,2048]{4,3,2,1,0:T(8,128)(2,1)} %copy.70), calls=%async_computation.1 | async-start | bytes 4194304 | tf_op jit(solution)/shard_map/all_to_all | solution.py:149
  318.8 28.0 %all-gather.3.cloned.1.call-start = ((), (), s32[]{:S(2)}) async-start(), calls=%async_computation.2 | async-start | bytes 2621440 | tf_op jit(solution)/shard_map/all_gather | solution.py:116
  322.2 1.3 copy-start.6
  322.2 1.6 copy-start.7
  369.0 9.1 %copy-start.1 = (bf16[2,256,2048]{2,1,0:T(8,128)(2,1)S(1)}, bf16[2,256,2048]{2,1,0:T(8,128)(2,1)}, u32[]{:S(2)}) copy-start(bf16[2,256,2048]{2,1,0:T(8,128)(2,1)} %param.25) | copy-start | bytes 6291460
Sparse Core Ops, SparseCore 0:
  77.6 57.2 all-gather.4
  156.3 152.8 all-reduce.2
  323.6 23.1 all-gather.2
where the time goes:
time: 385 us
  waiting for transfers between devices  239 us (62%)
  blocking collectives  55.5 us (14%)
  matrix products  30.1 us (8%)
  local copies, waits for them, and re-layouts  24.9 us (6%)
  between operations  14.1 us (4%)
  other arithmetic  11.5 us (3%)
  starting transfers between devices  9.2 us (2%)
    unnamed x4, waiting for transfers between devices  144 us
    all_gather x1, waiting for transfers between devices, per_device(): arrived = lax.all_gather(delivered, 'tp', axis=2, tiled=True)  57.4 us
    all_to_all x1, blocking collectives, per_device(): lax.all_to_all(buffer, 'ep', split_axis=0, concat_axis=0, tiled=True)  55.5 us
    all_gather x1, waiting for transfers between devices, per_device(): lax.all_gather(attended, 'tp', axis=1, tiled=True)  22.5 us
    all_to_all x1, waiting for transfers between devices, per_device(): lax.all_to_all(summed, 'ep', split_axis=0, concat_axis=0, tiled=True)  15.8 us
    dot_general x1, matrix products, per_device(): jnp.einsum('setcf,efd->setcd', activated, expert_down, preferred_element_...  13.5 us
  transfers between devices with their start and end apart: 5, of which 4 were waited for; matrix products, arithmetic and copies ran while one was open for 3% of the time, Pallas kernels for 0%

commit v1 on v0

--- a/solution.py
+++ b/solution.py
@@ -71,6 +71,22 @@
     expert_up,
     expert_down,
 ):
+
+    def time_knots(w_in, link_axis):
+        n_dev_all = jax.lax.axis_size(link_axis)
+        x_now = range(1, n_dev_all)
+        aux = map(lambda q: (q - 1, q), x_now)
+        extra = list(aux)
+        kept_arr = w_in
+        oldest = extra + [(n_dev_all - 1, 0)]
+        chunks = [kept_arr]
+        for _ in range(n_dev_all - 1):
+            kept_arr = jax.lax.ppermute(kept_arr, link_axis, oldest)
+            chunks += [kept_arr]
+        opened = jnp.concatenate([*reversed(chunks)], axis=2)
+        state_next = jax.lax.axis_index(link_axis)
+        return jnp.roll(opened, (state_next + 1) * kept_arr.shape[2], axis=2)
+
     span_len = WINDOW
     row_count = q_heads.shape[0]
     kv_local = k_heads.shape[1] // HD
@@ -131,7 +147,7 @@
     flat_routes, places = slot_positions(own_routes, 1, expert_count)
     buffer = fill_slots(own_normed, flat_routes, places, 1, expert_count, capacity, exp_local)
     delivered = lax.all_to_all(buffer, "ep", split_axis=0, concat_axis=0, tiled=True)
-    arrived = lax.all_gather(delivered, "tp", axis=2, tiled=True)
+    arrived = time_knots(delivered, "tp")
     own_flat = flat_routes[0]
     own_places = places[0]
     gates = gate_weights(own_normed, own_routes, router_group, router_expert)

time: 385 us -> 417 us (1.083)
  waiting for transfers between devices: 239 us -> 258 us
  local copies, waits for them, and re-layouts: 24.9 us -> 42.1 us
    ppermute x0 -> x3, waiting for transfers between devices: none -> 76.8 us  [time_knots(): kept_arr = jax.lax.ppermute(kept_arr, link_axis, oldest)]
    all_gather x1 -> x0, waiting for transfers between devices: 57.4 us -> none  [per_device(): arrived = lax.all_gather(delivered, 'tp', axis=2, tiled=True)]
    unnamed x27 -> x46, local copies, waits for them, and re-layouts: 5.8 us -> 24.1 us
    unnamed x4 -> x3, waiting for transfers between devices: 144 us -> 143 us
  transfers between devices with their start and end apart: 5 -> 7, of which waited for: 4 -> 6; matrix products, arithmetic and copies ran while one was open for 3% -> 3% of each run, Pallas kernels for 0% -> 0%
where the time goes in v1:
time: 417 us
  waiting for transfers between devices  258 us (62%)
  blocking collectives  55.5 us (13%)
  local copies, waits for them, and re-layouts  42.1 us (10%)
  matrix products  26.1 us (6%)
  between operations  14.5 us (3%)
  other arithmetic  11.5 us (3%)
  starting transfers between devices  9.16 us (2%)
    unnamed x3, waiting for transfers between devices  143 us
    ppermute x3, waiting for transfers between devices, time_knots(): kept_arr = jax.lax.ppermute(kept_arr, link_axis, oldest)  76.8 us
    all_to_all x1, blocking collectives, per_device(): lax.all_to_all(buffer, 'ep', split_axis=0, concat_axis=0, tiled=True)  55.5 us
    unnamed x46, local copies, waits for them, and re-layouts  24.1 us
    all_gather x1, waiting for transfers between devices, per_device(): lax.all_gather(attended, 'tp', axis=1, tiled=True)  22.5 us
    all_to_all x1, waiting for transfers between devices, per_device(): lax.all_to_all(summed, 'ep', split_axis=0, concat_axis=0, tiled=True)  15.8 us
    dot_general x1, matrix products, per_device(): jnp.einsum('setcf,efd->setcd', activated, expert_down, preferred_element_...  13.5 us
  transfers between devices with their start and end apart: 7, of which 6 were waited for; matrix products, arithmetic and copies ran while one was open for 3% of the time, Pallas kernels for 0%

profile of v1, /device:TPU:0, one launch (start us, length us, event | category | flops | bytes accessed | tf_op | source)
XLA Modules:
  0.0 416.7 jit_solution(13291510029330505890)
XLA Ops:
  13.8 2.3 reshape.383
  16.0 4.4 %scatter_custom_fusion = bf16[512,2048]{1,0:T(8,128)(2,1)} fusion(s32[256]{0:T(256)S(1)} %bitcast.169, bf16[256,2048]{1,0:T(8,128)(2,1)} %reshape.383, bf16[]{:T(256)} %constant.86.clone.1), kind=kCustom, calls=%fused_computation.36 | custom fusion | bytes 2097664 | tf_op jit(solution)/shard_map/scatter | solution.py:53
  20.5 55.5 %all_to_all.10 = bf16[8,2,1,32,2048]{4,3,2,1,0:T(8,128)(2,1)S(1)} all-to-all(bf16[8,2,1,32,2048]{4,3,2,1,0:T(8,128)(2,1)} %bitcast.157), channel_id=1, replica_groups=mesh['ep'=8,'tp'=4] {'ep'}, dimensions={0} | all-to-all | bytes 4194304 | tf_op jit(solution)/shard_map/all_to_all | solution.py:149
  77.6 25.4 %collective-permute-done.1 = bf16[8,2,1,32,2048]{4,3,2,0,1:T(8,128)(2,1)S(1)} collective-permute-done((bf16[8,2,1,32,2048]{4,3,2,0,1:T(8,128)(2,1)S(1)}, bf16[8,2,1,32,2048]{4,3,2,0,1:T(8,128)(2,1)S(1)}, u32[]{:S(2)}, u32[]{:S(2)}) %collective-permute-start.1) | collective-permute-done | bytes 2097184 | tf_op jit(solution)/shard_map/ppermute | solution.py:84
  104.4 25.6 %collective-permute-done.2 = bf16[8,2,1,32,2048]{4,3,2,0,1:T(8,128)(2,1)} collective-permute-done((bf16[8,2,1,32,2048]{4,3,2,0,1:T(8,128)(2,1)S(1)}, bf16[8,2,1,32,2048]{4,3,2,0,1:T(8,128)(2,1)}, u32[]{:S(2)}, u32[]{:S(2)}) %collective-permute-start.2) | collective-permute-done | bytes 2097184 | tf_op jit(solution)/shard_map/ppermute | solution.py:84
  130.0 25.8 %collective-permute-done.3 = bf16[8,2,1,32,2048]{4,3,2,0,1:T(8,128)(2,1)} collective-permute-done((bf16[8,2,1,32,2048]{4,3,2,0,1:T(8,128)(2,1)}, bf16[8,2,1,32,2048]{4,3,2,0,1:T(8,128)(2,1)}, u32[]{:S(2)}, u32[]{:S(2)}) %collective-permute-start.3) | collective-permute-done | bytes 2097184 | tf_op jit(solution)/shard_map/ppermute | solution.py:84
  155.7 1.8 constant_dynamic-update-slice_fusion.7
  157.6 2.0 constant_dynamic-update-slice_fusion.6
  161.5 1.8 constant_dynamic-update-slice_fusion.3
  163.4 1.8 constant_dynamic-update-slice_fusion.2
  165.5 6.1 %copy-done.10 = bf16[8,2,8,32,2048]{4,3,2,0,1:T(8,128)(2,1)} copy-done((bf16[8,2,8,32,2048]{4,3,2,0,1:T(8,128)(2,1)}, bf16[8,2,8,32,2048]{4,3,2,0,1:T(8,128)(2,1)S(1)}, u32[]{:S(2)}) %copy-start.10) | copy-done | bytes 16777240
  171.6 3.7 fusion.2
  175.3 13.5 %convert_bitcast_fusion = bf16[8,2,4,32,2048]{4,3,2,0,1:T(8,128)(2,1)} fusion(bf16[2,256,2048]{2,1,0:T(8,128)(2,1)S(1)} %copy-done, f32[2,8,4,32,256]{4,3,2,1,0:T(8,128)} %fusion.2, bf16[2,2048,256]{2,1,0:T(8,128)(2,1)} %param.24, bf16[8,2,8,32,2048]{4,3,2,0,1:T(8,128)(2,1)} %copy-done.10, s32[]{:T(128)S(6)} %select_n.54), kind=kOutput, calls=%fused_computation.2 | convolution fusion | flops 4302307328 | bytes 23068676 | tf_op jit(solution)/shard_map/setcf,efd->setcd/dot_general | solution.py:159
  189.8 3.5 collective-permute-start
  198.1 142.8 %all-reduce.3.cloned.1.call-done = bf16[8,2,4,32,2048]{4,3,2,0,1:T(8,128)(2,1)} async-done(((bf16[8,2,4,32,2048]{4,3,2,0,1:T(8,128)(2,1)}), bf16[8,2,4,32,2048]{4,3,2,0,1:T(8,128)(2,1)}) %all-reduce.3.cloned.1.call-update) | async-done | bytes 8388624
  340.9 2.5 constant_dynamic-slice_fusion.1
  345.0 5.5 %all-to-all-start.1 = ((bf16[8,2,1,32,2048]{4,3,2,1,0:T(8,128)(2,1)}), bf16[8,2,1,32,2048]{4,3,2,1,0:T(8,128)(2,1)S(1)}, u32[]{:S(2)}, u32[]{:S(2)}) async-start(bf16[8,2,1,32,2048]{4,3,2,1,0:T(8,128)(2,1)} %copy.74), calls=%async_computation.1 | async-start | bytes 4194304 | tf_op jit(solution)/shard_map/all_to_all | solution.py:165
  350.5 3.4 fusion.23
  356.0 22.5 %all-gather.2.cloned.1.call-done = bf16[1024,1024]{0,1:T(8,128)(2,1)} async-done(((bf16[1024,256]{0,1:T(8,128)(2,1)}), bf16[1024,1024]{0,1:T(8,128)(2,1)}) %all-gather.2.cloned.1.call-update) | async-done | bytes 2097168 | tf_op jit(solution)/shard_map/all_gather | solution.py:132
  378.5 4.1 convolution_convert_fusion
  382.6 15.8 %all-to-all-done.1 = bf16[8,2,1,32,2048]{4,3,2,1,0:T(8,128)(2,1)S(1)} async-done(((bf16[8,2,1,32,2048]{4,3,2,1,0:T(8,128)(2,1)}), bf16[8,2,1,32,2048]{4,3,2,1,0:T(8,128)(2,1)S(1)}, u32[]{:S(2)}, u32[]{:S(2)}) %all-to-all-start.1) | async-done | bytes 2097184 | tf_op jit(solution)/shard_map/all_to_all | solution.py:165
  398.4 2.3 gather_fusion
  400.7 3.5 reshape.370
  404.3 5.6 %multiply_reduce_fusion = bf16[128,2048]{1,0:T(8,128)(2,1)} fusion(f32[128,2,2048]{2,1,0:T(2,128)} %reshape.370, f32[128,2]{1,0:T(8,128)S(1)} %copy.64), kind=kLoop, calls=%fused_computation.24 | loop fusion | flops 786432 | bytes 2622464 | tf_op jit(solution)/shard_map/reduce_sum | solution.py:170
  (103 shorter events, 21.0 us)
Async XLA Ops:
  7.2 168.2 %copy-start = (bf16[2,256,2048]{2,1,0:T(8,128)(2,1)S(1)}, bf16[2,256,2048]{2,1,0:T(8,128)(2,1)}, u32[]{:S(2)}) copy-start(bf16[2,256,2048]{2,1,0:T(8,128)(2,1)} %param.25) | copy-start | bytes 6291460
  7.2 333.7 %all-reduce.3.cloned.1.call-start = ((), (), s32[]{:S(2)}) async-start(), calls=%async_computation.3 | async-start | bytes 16777216
  76.0 1.3 copy-start.2
  77.5 25.5 %collective-permute-start.1 = (bf16[8,2,1,32,2048]{4,3,2,0,1:T(8,128)(2,1)S(1)}, bf16[8,2,1,32,2048]{4,3,2,0,1:T(8,128)(2,1)S(1)}, u32[]{:S(2)}, u32[]{:S(2)}) collective-permute-start(bf16[8,2,1,32,2048]{4,3,2,0,1:T(8,128)(2,1)S(1)} %copy.71), channel_id=1, source_target_pairs={{0,1},{1,2},{2,3},{3,0},{4,5},{5,6},{6,7},{7,4},{8,9},{9,10},{10,1... | collective-permute-start | bytes 6291464 | tf_op jit(solution)/shard_map/ppermute | solution.py:84
  103.0 1.3 copy-start.4
  104.4 25.6 %collective-permute-start.2 = (bf16[8,2,1,32,2048]{4,3,2,0,1:T(8,128)(2,1)S(1)}, bf16[8,2,1,32,2048]{4,3,2,0,1:T(8,128)(2,1)}, u32[]{:S(2)}, u32[]{:S(2)}) collective-permute-start(bf16[8,2,1,32,2048]{4,3,2,0,1:T(8,128)(2,1)S(1)} %collective-permute-done.1), channel_id=1, source_target_pairs={{0,1},{1,2},{2,3},{3,0},{4,5},{5,6},{6,7},{7,4},{8,9},{9,10},{10,1... | collective-permute-start | bytes 6291464 | tf_op jit(solution)/shard_map/ppermute | solution.py:84
  130.0 25.8 %collective-permute-start.3 = (bf16[8,2,1,32,2048]{4,3,2,0,1:T(8,128)(2,1)}, bf16[8,2,1,32,2048]{4,3,2,0,1:T(8,128)(2,1)}, u32[]{:S(2)}, u32[]{:S(2)}) collective-permute-start(bf16[8,2,1,32,2048]{4,3,2,0,1:T(8,128)(2,1)} %collective-permute-done.2), channel_id=1, source_target_pairs={{0,1},{1,2},{2,3},{3,0},{4,5},{5,6},{6,7},{7,4},{8,9},{9,10},{10,1... | collective-permute-start | bytes 6291464 | tf_op jit(solution)/shard_map/ppermute | solution.py:84
  157.6 2.2 copy-start.5
  159.8 1.6 copy-start.3
  165.3 6.3 %copy-start.14 = (bf16[2,2048,256]{2,1,0:T(8,128)(2,1)S(1)}, bf16[2,2048,256]{2,1,0:T(8,128)(2,1)}, u32[]{:S(2)}) copy-start(bf16[2,2048,256]{2,1,0:T(8,128)(2,1)} %param.23) | copy-start | bytes 6291460
  165.5 6.1 %copy-start.10 = (bf16[8,2,8,32,2048]{4,3,2,0,1:T(8,128)(2,1)}, bf16[8,2,8,32,2048]{4,3,2,0,1:T(8,128)(2,1)S(1)}, u32[]{:S(2)}) copy-start(bf16[8,2,8,32,2048]{4,3,2,0,1:T(8,128)(2,1)S(1)} %constant_dynamic-update-slice_fusion) | copy-start | bytes 50331652
  188.8 0.9 copy-start.7
  188.8 1.0 copy-start.8
  188.8 5.0 %copy-start.9 = (bf16[1024,256]{1,0:T(8,128)(2,1)S(1)}, bf16[1024,256]{1,0:T(8,128)(2,1)}, u32[]{:S(2)}) copy-start(bf16[1024,256]{1,0:T(8,128)(2,1)} %param.13) | copy-start | bytes 1572868
  189.8 4.6 %copy-start.15 = (u32[32]{0:T(128)S(1)}, u32[32]{0:T(128)}, u32[]{:S(2)}) copy-start(u32[32]{0:T(128)} %constant.96) | copy-start | bytes 388
  189.8 5.2 %collective-permute-start = (bf16[2,128,64]{1,2,0:T(8,128)(2,1)S(1)}, bf16[2,128,64]{1,2,0:T(8,128)(2,1)S(1)}, u32[]{:S(2)}, u32[]{:S(2)}) collective-permute-start(bf16[2,128,64]{1,2,0:T(8,128)(2,1)S(1)} %pad_maximum_fusion.2), channel_id=1, source_target_pairs={{0,4},{4,8},{8,12},{12,16},{16,20},{20,24},{24,28},{1,5},{5,9},{9,... | collective-permute-start | bytes 98312 | tf_op jit(solution)/shard_map/ppermute | solution.py:15
  195.1 0.9 copy-start.13
  196.0 2.0 copy-start.6
  345.0 53.4 %all-to-all-start.1 = ((bf16[8,2,1,32,2048]{4,3,2,1,0:T(8,128)(2,1)}), bf16[8,2,1,32,2048]{4,3,2,1,0:T(8,128)(2,1)S(1)}, u32[]{:S(2)}, u32[]{:S(2)}) async-start(bf16[8,2,1,32,2048]{4,3,2,1,0:T(8,128)(2,1)} %copy.74), calls=%async_computation.1 | async-start | bytes 4194304 | tf_op jit(solution)/shard_map/all_to_all | solution.py:165
  350.5 28.0 %all-gather.2.cloned.1.call-start = ((), (), s32[]{:S(2)}) async-start(), calls=%async_computation.2 | async-start | bytes 2621440 | tf_op jit(solution)/shard_map/all_gather | solution.py:132
  353.9 1.3 copy-start.11
  353.9 1.6 copy-start.12
  400.7 9.1 %copy-start.1 = (bf16[2,256,2048]{2,1,0:T(8,128)(2,1)S(1)}, bf16[2,256,2048]{2,1,0:T(8,128)(2,1)}, u32[]{:S(2)}) copy-start(bf16[2,256,2048]{2,1,0:T(8,128)(2,1)} %param.25) | copy-start | bytes 6291460
Sparse Core Ops, SparseCore 0:
  189.0 151.8 all-reduce.2
  355.3 23.1 all-gather.1
